TPU v7x, 32 devices: a whole 2x2x4 slice. The times are simulated.
32 devices in a mesh: fs: 4 (over y, x), tp: 8 (over z, core).
Axes of the slice: x: 2, y: 2, z: 4, core: 2. Of those that a mesh axis runs over, the one named last changes fastest.
Arguments:
- tokens_in: bfloat16 [8192, 2048], P(('fs', 'tp')), may hold values from -6 to 6
- gate_cotangent: bfloat16 [8192, 1024], P(('fs', 'tp')), may hold values from -0.125 to 0.125
- conv_output: bfloat16 [8192, 1024], P(('fs', 'tp')), may hold values from -6 to 6
- block_cotangent: bfloat16 [8192, 2048], P(('fs', 'tp')), may hold values from -0.125 to 0.125
- projectors: bfloat16 [2048, 2, 256], P('fs'), may hold values from -0.125 to 0.125
- first_moment: float32 [256, 2, 1024], P('fs', None, 'tp'), may hold values from -6 to 6
- second_moment: float32 [256, 2, 1024], P('fs', None, 'tp'), may hold values from 0.25 to 4
- gate_master: float32 [2048, 1024], P('fs', 'tp'), may hold values from -0.125 to 0.125
- out_master: float32 [1024, 2048], P('tp', 'fs'), may hold values from -0.1875 to 0.1875
Outputs:
- first_new: float32 [256, 2, 1024], P('fs', None, 'tp')
- second_new: float32 [256, 2, 1024], P('fs', None, 'tp')
- step_gate: float32 [2048, 1024], P('fs', 'tp')
- step_out: float32 [1024, 2048], P('tp', 'fs')
- gate_new: float32 [2048, 1024], P('fs', 'tp')
- out_new: float32 [1024, 2048], P('tp', 'fs')
- gate_copy: bfloat16 [2048, 1024], P(None, 'tp')
- out_copy: bfloat16 [1024, 2048], P('tp')
All inputs are finite; a program needn't handle non-finite values.
Results may differ from a plain program's by a relative error of at most 0.0035.
Values may be sent and summed in bfloat16 or wider, within the bound.
A program may use at most 64 MiB of HBM per device.

v0:
```python
import math

import jax
import jax.numpy as jnp
from jax import lax
from jax.sharding import PartitionSpec as P

CH = 1024
RANK = 256


BETA_FIRST = 0.8
BETA_SECOND = 0.9
LEARN_RATE = 0.01
CLIP_SHARE = 0.5
HIGHEST_MODE = lax.Precision.HIGHEST


def tiled_rows(row_start, row_count, inner_rows, tile_total, builder):
    tile_span = inner_rows * tile_total
    shaped = builder(row_start // tile_span, row_count // tile_span, 0, tile_total)
    return shaped.reshape(row_count, 2, shaped.shape[-1])


def tile_product(left_rows, right_cols, tile_count, width_cols):
    right_part = right_cols
    right_part = right_part.reshape(right_part.shape[0], tile_count, width_cols)
    return jnp.einsum("raq,rtc->atqc", left_rows, right_part, preferred_element_type=jnp.float32)


def split_product(mixed_rows, right_cols, tile_count, width_cols):
    upper_part = lax.optimization_barrier(mixed_rows.astype(jnp.bfloat16))
    lower_part = (mixed_rows - upper_part.astype(jnp.float32)).astype(jnp.bfloat16)
    return tile_product(upper_part, right_cols, tile_count, width_cols) + tile_product(
        lower_part, right_cols, tile_count, width_cols
    )


def shards(
    tokens_in,
    gate_cotangent,
    conv_output,
    block_cotangent,
    projectors,
    first_moment,
    second_moment,
    gate_master,
    out_master,
):
    tile_total = lax.axis_size("tp")
    local_rows = tokens_in.shape[0]
    width_cols = gate_master.shape[1]
    rank_rows = first_moment.shape[0]
    own_proj = projectors.astype(jnp.float32)
    whole_proj = lax.all_gather(projectors, "fs", axis=0, tiled=True)

    def low_blocks(first_block, block_count, first_tile, tile_count):
        gate_mix = jnp.dot(tokens_in, whole_proj[:, 0, :], preferred_element_type=jnp.float32)
        flip_mix = jnp.dot(block_cotangent, whole_proj[:, 1, :], preferred_element_type=jnp.float32)
        gate_mix = gate_mix.reshape(local_rows, block_count, rank_rows)
        flip_mix = flip_mix.reshape(local_rows, block_count, rank_rows)
        gate_term = split_product(gate_mix, gate_cotangent, tile_count, width_cols)
        flip_term = split_product(flip_mix, conv_output, tile_count, width_cols)
        return jnp.stack((gate_term, flip_term), axis=3)

    low_space = lax.psum_scatter(
        tiled_rows(
            jnp.int32(0), rank_rows * lax.axis_size(("fs", "tp")), rank_rows, tile_total, low_blocks
        ),
        ("fs", "tp"),
        scatter_dimension=0,
        tiled=True,
    )
    first_new = BETA_FIRST * first_moment + (1.0 - BETA_FIRST) * low_space
    second_new = BETA_SECOND * second_moment + (1.0 - BETA_SECOND) * low_space * low_space
    direction = first_new / jnp.sqrt(second_new)
    squares = jnp.sum(direction * direction, axis=(0, 2))
    global_sums = lax.psum(squares, ("fs", "tp"))
    clip_level = CLIP_SHARE * math.sqrt(RANK * CH)
    factor = clip_level / jnp.maximum(jnp.sqrt(global_sums), clip_level)
    raw_step = jnp.einsum(
        "dmr,rmc->dmc",
        own_proj,
        lax.all_gather(direction, "fs", axis=0, tiled=True),
        precision=HIGHEST_MODE,
    )
    scaled_step = raw_step * factor[None, :, None]
    step_gate = scaled_step[:, 0, :]
    step_out = scaled_step[:, 1, :].T
    gate_new = gate_master - LEARN_RATE * step_gate
    out_new = out_master - LEARN_RATE * step_out
    gate_copy, out_copy = (
        lax.all_gather(gate_new.astype(jnp.bfloat16), "fs", axis=0, tiled=True),
        lax.all_gather(out_new.astype(jnp.bfloat16), "fs", axis=1, tiled=True),
    )
    return (first_new, second_new, step_gate, step_out, gate_new, out_new, gate_copy, out_copy)


def solution(mesh):
    in_specs = (
        P(("fs", "tp"), None),
        P(("fs", "tp"), None),
        P(("fs", "tp"), None),
        P(("fs", "tp"), None),
        P("fs", None, None),
        P("fs", None, "tp"),
        P("fs", None, "tp"),
        P("fs", "tp"),
        P("tp", "fs"),
    )
    out_specs = (
        P("fs", None, "tp"),
        P("fs", None, "tp"),
        P("fs", "tp"),
        P("tp", "fs"),
        P("fs", "tp"),
        P("tp", "fs"),
        P(None, "tp"),
        P("tp", None),
    )
    return jax.shard_map(shards, mesh=mesh, in_specs=in_specs, out_specs=out_specs, check_vma=False)
```

profile of v0, /device:TPU:0, one launch (start us, length us, event | category | flops | bytes accessed | tf_op | source)
XLA Modules:
  0.0 278.2 jit_solution(3565920603312348858)
XLA Ops:
  7.2 0.0 copy-start
  7.2 0.0 all-gather.2.cloned.1.call-start
  7.2 2.0 copy.33
  9.2 0.0 all-gather.2.cloned.1.call-update
  9.2 0.0 reduce-scatter.2.cloned.1.call-start
  9.3 39.1 %all-gather.2.cloned.1.call-done = bf16[2048,2,256]{2,0,1:T(8,128)(2,1)} async-done(((bf16[512,2,256]{2,0,1:T(8,128)(2,1)}), bf16[2048,2,256]{2,0,1:T(8,128)(2,1)}) %all-gather.2.cloned.1.call-update) | async-done | bytes 2097168 | tf_op jit(solution)/shard_map/all_gather | solution.py:55
  48.3 2.7 slice_bitcast_fusion.1
  51.0 1.5 copy.34
  52.5 0.0 copy-done
  52.5 0.5 fusion.25
  53.0 0.6 copy.37
  53.6 0.0 copy-start.2
  53.7 1.8 fusion.24
  55.4 0.0 copy-done.2
  55.4 0.0 copy-start.3
  55.4 0.3 fusion.6
  55.7 0.3 convolution_add_fusion.1
  56.1 0.4 copy-done.3
  56.5 0.3 fusion.5
  56.8 0.3 convolution_add_fusion
  57.1 1.5 pad_maximum_fusion
  58.6 0.0 copy-start.4
  58.6 0.0 copy-start.6
  58.6 0.0 copy-start.7
  58.6 0.0 copy-start.1
  58.6 0.0 copy-start.5
  58.6 0.0 reduce-scatter.2.cloned.1.call-update
  58.6 0.9 copy-done.4
  59.5 0.1 copy.42
  59.6 138.0 %reduce-scatter.2.cloned.1.call-done = f32[64,2,128]{2,0,1:T(8,128)} async-done(((f32[2048,2,128]{2,0,1:T(8,128)}), f32[64,2,128]{2,0,1:T(8,128)}) %reduce-scatter.2.cloned.1.call-update) | async-done | bytes 65552 | tf_op jit(solution)/shard_map/reduce_scatter | solution.py:66
  197.6 0.0 copy-done.6
  197.6 0.0 copy-done.7
  197.6 1.0 multiply_reduce_fusion
  198.6 8.1 %all_gather.13 = f32[256,2,128]{2,0,1:T(8,128)S(1)} all-gather(f32[64,2,128]{2,0,1:T(8,128)S(1)} %get-tuple-element.30), channel_id=1, replica_groups=mesh['fs'=4,'tp'=8] {'fs'}, dimensions={0}, use_global_device_ids=true | all-gather | bytes 327680 | tf_op jit(solution)/shard_map/all_gather | solution.py:84
  206.6 36.8 %psum.7 = f32[2]{0:T(128)S(1)} all-reduce(f32[2]{0:T(128)S(1)} %get-tuple-element.29), channel_id=1, replica_groups=mesh['fs'=4,'tp'=8] {'fs','tp'}, use_global_device_ids=true, to_apply=%region_2.0 | all-reduce | flops 2 | bytes 16 | tf_op jit(solution)/shard_map/psum | solution.py:78
  243.4 0.0 copy-done.1
  243.4 0.7 fusion
  244.2 0.0 copy-done.5
  244.2 0.8 fusion.20
  245.0 11.5 %all_gather.15 = bf16[128,2048]{1,0:T(8,128)(2,1)S(1)} all-gather(bf16[128,512]{1,0:T(8,128)(2,1)S(1)} %get-tuple-element.24), channel_id=1, replica_groups=mesh['fs'=4,'tp'=8] {'fs'}, dimensions={1}, use_global_device_ids=true | all-gather | bytes 655360 | tf_op jit(solution)/shard_map/all_gather | solution.py:94
  256.6 10.0 %all_gather.14 = bf16[2048,128]{0,1:T(8,128)(2,1)S(1)} all-gather(bf16[512,128]{0,1:T(8,128)(2,1)S(1)} %get-tuple-element.27), channel_id=1, replica_groups=mesh['fs'=4,'tp'=8] {'fs'}, dimensions={0}, use_global_device_ids=true | all-gather | bytes 655360 | tf_op jit(solution)/shard_map/all_gather | solution.py:93
  266.5 1.0 copy.47
  267.5 0.8 copy.46
  268.4 0.8 copy.45
  269.2 0.7 copy.43
  269.9 0.7 copy.44
  270.6 0.8 copy.81
  (3 shorter events, 0.1 us)
Async XLA Ops:
  7.2 45.3 %copy-start = (bf16[256,2048]{1,0:T(8,128)(2,1)S(1)}, bf16[256,2048]{1,0:T(8,128)(2,1)}, u32[]{:S(2)}) copy-start(bf16[256,2048]{1,0:T(8,128)(2,1)} %param.9) | copy-start | bytes 3145732
  7.2 41.2 %all-gather.2.cloned.1.call-start = ((), (), s32[]{:S(2)}) async-start(), calls=%async_computation.1 | async-start | bytes 2621440 | tf_op jit(solution)/shard_map/all_gather | solution.py:55
  9.2 188.4 %reduce-scatter.2.cloned.1.call-start = ((), (), s32[]{:S(2)}) async-start(), calls=%async_computation.2 | async-start | bytes 2162688 | tf_op jit(solution)/shard_map/reduce_scatter | solution.py:66
  53.6 1.8 copy-start.2
  55.4 1.0 copy-start.3
  58.6 0.9 copy-start.4
  58.6 139.0 %copy-start.6 = (f32[64,2,128]{2,1,0:T(2,128)S(1)}, f32[64,2,128]{2,1,0:T(2,128)}, u32[]{:S(2)}) copy-start(f32[64,2,128]{2,1,0:T(2,128)} %param.15) | copy-start | bytes 196612
  58.6 139.0 %copy-start.7 = (f32[64,2,128]{2,1,0:T(2,128)S(1)}, f32[64,2,128]{2,1,0:T(2,128)}, u32[]{:S(2)}) copy-start(f32[64,2,128]{2,1,0:T(2,128)} %param.14) | copy-start | bytes 196612
  58.6 184.9 %copy-start.1 = (bf16[512,2,256]{2,1,0:T(2,128)(2,1)S(1)}, bf16[512,2,256]{2,1,0:T(2,128)(2,1)}, u32[]{:S(2)}) copy-start(bf16[512,2,256]{2,1,0:T(2,128)(2,1)} %param.13) | copy-start | bytes 1572868
  58.6 185.6 %copy-start.5 = (f32[128,512]{1,0:T(8,128)S(1)}, f32[128,512]{1,0:T(8,128)}, u32[]{:S(2)}) copy-start(f32[128,512]{1,0:T(8,128)} %param.17) | copy-start | bytes 786436
Sparse Core Ops, SparseCore 0:
  10.4 37.8 all-gather.1
  58.7 138.8 reduce-scatter.1
where the time goes:
time: 279 us; the launch traced here: 278 us
  waiting for transfers between devices  177 us (63%)
  blocking collectives  66.3 us (24%)
  between operations  14.2 us (5%)
  local copies, waits for them, and re-layouts  13.1 us (5%)
  matrix products  4.14 us (1%)
  other arithmetic  3.33 us (1%)
    reduce_scatter x1, waiting for transfers between devices, shards(): lax.psum_scatter(tiled_rows(jnp.int32(0), rank_rows * lax.axis_size(('fs'...  138 us
    all_gather x1, waiting for transfers between devices, shards(): whole_proj = lax.all_gather(projectors, 'fs', axis=0, tiled=True)  39.1 us
    psum x1, blocking collectives, shards(): global_sums = lax.psum(squares, ('fs', 'tp'))  36.8 us
    all_gather x1, blocking collectives, shards(): lax.all_gather(out_new.astype(jnp.bfloat16), 'fs', axis=1, tiled=True)  11.5 us
    all_gather x1, blocking collectives, shards(): lax.all_gather(gate_new.astype(jnp.bfloat16), 'fs', axis=0, tiled=True)  9.96 us
    unnamed x24, local copies, waits for them, and re-layouts  8.29 us
    all_gather x1, blocking collectives, shards(): lax.all_gather(direction, 'fs', axis=0, tiled=True)  8.06 us
  transfers between devices with their start and end apart: 2, of which 2 were waited for; matrix products, arithmetic and copies ran while one was open for 0% of the time, Pallas kernels for 0%

commit v1 on v0

v1 whole, which is shorter than its diff:
```python
import functools
import math

import jax
import jax.numpy as jnp
from jax import lax
from jax.experimental import pallas as pl
from jax.experimental.pallas import tpu as pltpu
from jax.sharding import PartitionSpec as P

BETA_FIRST = 0.8
BETA_SECOND = 0.9
LEARN_RATE = 0.01
CLIP_SHARE = 0.5
MESH_ID = pl.DeviceIdType.MESH
WIDE = jnp.float32
SLIM = jnp.bfloat16


def update_kernel(
    fs_total,
    tp_total,
    clip_level,
    tokens_in,
    gate_cot,
    conv_out,
    block_cot,
    proj,
    first_old,
    second_old,
    gate_old,
    out_old,
    first_new,
    second_new,
    step_gate,
    step_out,
    gate_new,
    out_new,
    gate_copy,
    out_copy,
    left,
    right,
    peers_proj,
    mix,
    low,
    fs_out,
    fs_in,
    tile_sum,
    tp_out,
    tp_in,
    dirs,
    squares,
    swap_send,
    swap_recv,
    load_sem,
    proj_send,
    proj_recv,
    fs_send,
    fs_recv,
    tp_send,
    tp_recv,
    dir_send,
    dir_recv,
    square_send,
    square_recv,
    gate_send,
    gate_recv,
    out_send,
    out_recv,
):
    me_fs = lax.axis_index("fs")
    me_tp = lax.axis_index("tp")
    core = lax.rem(me_tp, 2)
    partner = me_tp + 1 - 2 * core
    rows_d, rank = proj.shape[1], proj.shape[2]
    rank_rows = rank // fs_total
    width = gate_old.shape[1]
    local = tokens_in.shape[0]

    def fs_peer(step):
        return lax.rem(me_fs + step, fs_total)

    def fs_source(step):
        return lax.rem(me_fs + fs_total - step, fs_total)

    def tp_peer(step):
        return lax.rem(me_tp + step, tp_total)

    def send_fs(source, target, send_sem, recv_sem, step):
        return pltpu.make_async_remote_copy(
            src_ref=source,
            dst_ref=target,
            send_sem=send_sem.at[step],
            recv_sem=recv_sem.at[step],
            device_id={"fs": fs_peer(step), "tp": me_tp},
            device_id_type=MESH_ID,
        )

    def send_tp(source, target, send_sem, recv_sem, step, target_tp):
        return pltpu.make_async_remote_copy(
            src_ref=source,
            dst_ref=target,
            send_sem=send_sem.at[step],
            recv_sem=recv_sem.at[step],
            device_id={"fs": me_fs, "tp": target_tp},
            device_id_type=MESH_ID,
        )

    def own_copy(source, target, slot):
        return pltpu.make_async_copy(source, target, load_sem.at[slot])

    @pl.when(core == 0)
    def _():
        own_copy(tokens_in, left.at[0], 0).start()
        own_copy(gate_cot, right.at[0], 1).start()

    @pl.when(core == 1)
    def _():
        own_copy(block_cot, left.at[0], 0).start()
        own_copy(conv_out, right.at[0], 1).start()

    barrier = pltpu.get_barrier_semaphore()
    for step in range(1, fs_total):
        pl.semaphore_signal(
            barrier, inc=1, device_id={"fs": fs_peer(step), "tp": me_tp}, device_id_type=MESH_ID
        )
    for step in range(1, tp_total):
        pl.semaphore_signal(
            barrier, inc=1, device_id={"fs": me_fs, "tp": tp_peer(step)}, device_id_type=MESH_ID
        )
    pl.semaphore_wait(barrier, fs_total + tp_total - 2)

    proj_copies = [None]
    for step in range(1, fs_total):
        copy = send_fs(proj.at[core], peers_proj.at[step], proj_send, proj_recv, step)
        copy.start()
        proj_copies.append(copy)

    swap_left = send_tp(block_cot, left.at[1], swap_send, swap_recv, 0, partner)
    swap_right = send_tp(conv_out, right.at[1], swap_send, swap_recv, 1, partner)

    @pl.when(core == 0)
    def _():
        swap_left.start()
        swap_right.start()

    @pl.when(core == 1)
    def _():
        send_tp(tokens_in, left.at[1], swap_send, swap_recv, 0, partner).start()
        send_tp(gate_cot, right.at[1], swap_send, swap_recv, 1, partner).start()

    own_copy(tokens_in, left.at[0], 0).wait()
    swap_left.wait_recv()

    def mixed(block, factor_rows):
        columns = pl.ds(pl.multiple_of(block * rows_d, 128), rows_d)
        part = left[:, :, columns].reshape(2 * local, rows_d)
        return jnp.dot(part, factor_rows, preferred_element_type=WIDE)

    mix[...] = mixed(me_fs, proj[core])
    for step in range(1, fs_total):
        proj_copies[step].wait_recv()
        mix[...] += mixed(fs_source(step), peers_proj[step])

    own_copy(gate_cot, right.at[0], 1).wait()
    swap_right.wait_recv()
    upper = mix[...].astype(SLIM)
    lower = (mix[...] - upper.astype(WIDE)).astype(SLIM)
    cots = right[...].reshape(2 * local, right.shape[2])
    dims = (((0,), (0,)), ((), ()))
    low[...] = lax.dot_general(upper, cots, dims, preferred_element_type=WIDE) + lax.dot_general(
        lower, cots, dims, preferred_element_type=WIDE
    )

    def low_rows(block):
        return low[pl.ds(pl.multiple_of(block * rank_rows, 8), rank_rows), :]

    fs_copies = [None]
    for step in range(1, fs_total):
        rows = low_rows(fs_peer(step)).astype(SLIM)
        for tile in range(tp_total):
            fs_out[step, tile] = rows[:, tile * width : (tile + 1) * width]
        copy = send_fs(fs_out.at[step], fs_in.at[step], fs_send, fs_recv, step)
        copy.start()
        fs_copies.append(copy)
    rows = low_rows(me_fs)
    for tile in range(tp_total):
        tile_sum[tile] = rows[:, tile * width : (tile + 1) * width]
    for step in range(1, fs_total):
        fs_copies[step].wait_recv()
        tile_sum[...] += fs_in[step].astype(WIDE)

    tp_copies = [None]
    for step in range(1, tp_total):
        tp_out[step] = tile_sum[tp_peer(step)].astype(SLIM)
        copy = send_tp(tp_out.at[step], tp_in.at[step], tp_send, tp_recv, step, tp_peer(step))
        copy.start()
        tp_copies.append(copy)
    same = tile_sum[me_tp]
    other = None
    for step in range(1, tp_total):
        tp_copies[step].wait_recv()
        piece = tp_in[step].astype(WIDE)
        if step % 2 == 0:
            same = same + piece
        else:
            other = piece if other is None else other + piece

    lows = (jnp.where(core == 0, same, other), jnp.where(core == 0, other, same))
    for index in range(2):
        picked = pl.ds(index, rank_rows, stride=2)
        first = BETA_FIRST * first_old[picked, :] + (1.0 - BETA_FIRST) * lows[index]
        second = BETA_SECOND * second_old[picked, :] + (1.0 - BETA_SECOND) * lows[index] * lows[index]
        first_new[picked, :] = first
        second_new[picked, :] = second
        dirs[me_fs, index] = (first / jnp.sqrt(second)).astype(SLIM)

    dir_copies = [None]
    for step in range(1, fs_total):
        copy = send_fs(dirs.at[me_fs], dirs.at[me_fs], dir_send, dir_recv, step)
        copy.start()
        dir_copies.append(copy)
    for step in range(1, fs_total):
        dir_copies[step].wait_recv()

    gate_dir = dirs[:, 0].reshape(rank, width)
    flip_dir = dirs[:, 1].reshape(rank, width)
    gate_wide = gate_dir.astype(WIDE)
    flip_wide = flip_dir.astype(WIDE)
    squares[0, 0] = jnp.sum((gate_wide * gate_wide).reshape(rank // 8, 8, width), axis=0)
    squares[0, 1] = jnp.sum((flip_wide * flip_wide).reshape(rank // 8, 8, width), axis=0)
    square_copies = [None]
    for step in range(1, tp_total):
        copy = send_tp(
            squares.at[0], squares.at[step], square_send, square_recv, step, tp_peer(step)
        )
        copy.start()
        square_copies.append(copy)
    raw_gate = jnp.dot(proj[0], gate_dir, preferred_element_type=WIDE)
    raw_out = lax.dot_general(
        flip_dir, proj[1], (((0,), (1,)), ((), ())), preferred_element_type=WIDE
    )
    for step in range(1, tp_total):
        square_copies[step].wait_recv()
    totals = jnp.sum(squares[...], axis=0)
    gate_norm = jnp.sqrt(jnp.sum(totals[0], keepdims=True))
    flip_norm = jnp.sqrt(jnp.sum(totals[1], keepdims=True))
    scaled_gate = raw_gate * (clip_level / jnp.maximum(gate_norm, clip_level))
    scaled_out = raw_out * (clip_level / jnp.maximum(flip_norm, clip_level))
    step_gate[...] = scaled_gate
    step_out[...] = scaled_out
    fresh_gate = gate_old[...] - LEARN_RATE * scaled_gate
    fresh_out = out_old[...] - LEARN_RATE * scaled_out
    own_rows = pl.ds(pl.multiple_of(me_fs * rows_d, 128), rows_d)
    gate_copy[own_rows, :] = fresh_gate.astype(SLIM)
    out_copy[:, own_rows] = fresh_out.astype(SLIM)
    gate_block = gate_copy.at[own_rows, :]
    out_block = out_copy.at[:, own_rows]
    last_copies = []
    for step in range(1, fs_total):
        copy = send_fs(gate_block, gate_block, gate_send, gate_recv, step)
        copy.start()
        last_copies.append(copy)
        copy = send_fs(out_block, out_block, out_send, out_recv, step)
        copy.start()
        last_copies.append(copy)
    gate_new[...] = fresh_gate
    out_new[...] = fresh_out
    for step in range(1, fs_total):
        proj_copies[step].wait_send()
        fs_copies[step].wait_send()
        dir_copies[step].wait_send()
    for step in range(1, tp_total):
        tp_copies[step].wait_send()
        square_copies[step].wait_send()
    swap_left.wait_send()
    swap_right.wait_send()
    for copy in last_copies:
        copy.wait()


def shards(
    tokens_in,
    gate_cotangent,
    conv_output,
    block_cotangent,
    projectors,
    first_moment,
    second_moment,
    gate_master,
    out_master,
):
    fs_total = lax.axis_size("fs")
    tp_total = lax.axis_size("tp")
    local, model = tokens_in.shape
    channels = gate_cotangent.shape[1]
    rows_d, _, rank = projectors.shape
    rank_rows, _, width = first_moment.shape
    clip_level = CLIP_SHARE * math.sqrt(rank * channels)
    proj = jnp.transpose(projectors, (1, 0, 2))
    flat = (2 * rank_rows, width)
    shape = jax.ShapeDtypeStruct
    whole = pl.BlockSpec(memory_space=pltpu.VMEM)
    away = pl.BlockSpec(memory_space=pl.ANY)
    fs_sems = pltpu.SemaphoreType.DMA((fs_total,))
    tp_sems = pltpu.SemaphoreType.DMA((tp_total,))
    two_sems = pltpu.SemaphoreType.DMA((2,))
    results = pl.pallas_call(
        functools.partial(update_kernel, fs_total, tp_total, clip_level),
        out_shape=(
            shape(flat, WIDE),
            shape(flat, WIDE),
            shape((rows_d, width), WIDE),
            shape((width, rows_d), WIDE),
            shape((rows_d, width), WIDE),
            shape((width, rows_d), WIDE),
            shape((model, width), SLIM),
            shape((width, model), SLIM),
        ),
        in_specs=[away] * 4 + [whole] * 5,
        out_specs=(whole,) * 8,
        scratch_shapes=[
            pltpu.VMEM((2, local, model), SLIM),
            pltpu.VMEM((2, local, channels), SLIM),
            pltpu.VMEM((fs_total, rows_d, rank), SLIM),
            pltpu.VMEM((2 * local, rank), WIDE),
            pltpu.VMEM((rank, channels), WIDE),
            pltpu.VMEM((fs_total, tp_total, rank_rows, width), SLIM),
            pltpu.VMEM((fs_total, tp_total, rank_rows, width), SLIM),
            pltpu.VMEM((tp_total, rank_rows, width), WIDE),
            pltpu.VMEM((tp_total, rank_rows, width), SLIM),
            pltpu.VMEM((tp_total, rank_rows, width), SLIM),
            pltpu.VMEM((fs_total, 2, rank_rows, width), SLIM),
            pltpu.VMEM((tp_total, 2, 8, width), WIDE),
            two_sems,
            two_sems,
            two_sems,
            fs_sems,
            fs_sems,
            fs_sems,
            fs_sems,
            tp_sems,
            tp_sems,
            fs_sems,
            fs_sems,
            tp_sems,
            tp_sems,
            fs_sems,
            fs_sems,
            fs_sems,
            fs_sems,
        ],
        compiler_params=pltpu.CompilerParams(
            collective_id=0, has_side_effects=True, vmem_limit_bytes=40 * 1024 * 1024
        ),
    )(
        tokens_in,
        gate_cotangent,
        conv_output,
        block_cotangent,
        proj,
        first_moment.reshape(flat),
        second_moment.reshape(flat),
        gate_master,
        out_master,
    )
    first_new, second_new = (part.reshape(rank_rows, 2, width) for part in results[:2])
    return (first_new, second_new) + tuple(results[2:])


def solution(mesh):
    in_specs = (
        P(("fs", "tp"), None),
        P(("fs", "tp"), None),
        P(("fs", "tp"), None),
        P(("fs", "tp"), None),
        P("fs", None, None),
        P("fs", None, "tp"),
        P("fs", None, "tp"),
        P("fs", "tp"),
        P("tp", "fs"),
    )
    out_specs = (
        P("fs", None, "tp"),
        P("fs", None, "tp"),
        P("fs", "tp"),
        P("tp", "fs"),
        P("fs", "tp"),
        P("tp", "fs"),
        P(None, "tp"),
        P("tp", None),
    )
    return jax.shard_map(shards, mesh=mesh, in_specs=in_specs, out_specs=out_specs, check_vma=False)
```

time: 279 us -> 69.4 us (0.25)
  waiting for transfers between devices: 177 us -> 0 us
  blocking collectives: 66.3 us -> 0 us
  Pallas kernels: 0 us -> 54.3 us
  between operations: 14.2 us -> 0.66 us
  matrix products: 4.14 us -> 0 us
  other arithmetic: 3.33 us -> 0 us
    reduce_scatter x1 -> x0, waiting for transfers between devices: 138 us -> none  [shards(): lax.psum_scatter(tiled_rows(jnp.int32(0), rank_rows * lax.axis_size(('fs'...]
    pallas_call x0 -> x1, Pallas kernels: none -> 54.3 us  [shards(): pl.pallas_call(functools.partial(update_kernel, fs_total, tp_total, clip_...]
    all_gather x1 -> x0, waiting for transfers between devices: 39.1 us -> none  [shards(): whole_proj = lax.all_gather(projectors, 'fs', axis=0, tiled=True)]
    psum x1 -> x0, blocking collectives: 36.8 us -> none  [shards(): global_sums = lax.psum(squares, ('fs', 'tp'))]
    all_gather x3 -> x0, blocking collectives: 29.5 us -> none  [the longest x1 11.5 us: shards(): lax.all_gather(out_new.astype(jnp.bfloat16), 'fs', axis=1, tiled=True)]
    unnamed x24 -> x25, local copies, waits for them, and re-layouts: 8.29 us -> 13.9 us
    dot_general x3 -> x0, local copies, waits for them, and re-layouts: 4.79 us -> none  [the longest x2 4.15 us: low_blocks(): jnp.dot(tokens_in, whole_proj[:, 0, :], preferred_element_type=jnp.float32)]
    dot_general x7 -> x0, matrix products: 4.14 us -> none  [the longest x1 1.75 us: low_blocks(): jnp.dot(block_cotangent, whole_proj[:, 1, :], preferred_element_type=jnp....]
  transfers between devices with their start and end apart: 2 -> 0, of which waited for: 2 -> 0; matrix products, arithmetic and copies ran while one was open for 0% -> 0% of each run, Pallas kernels for 0% -> 0%
where the time goes in v1:
time: 69.4 us; the launch traced here: 68.9 us
  Pallas kernels  54.3 us (78%)
  local copies, waits for them, and re-layouts  13.9 us (20%)
    pallas_call x1, Pallas kernels, shards(): pl.pallas_call(functools.partial(update_kernel, fs_total, tp_total, clip_...  54.3 us
    unnamed x25, local copies, waits for them, and re-layouts  13.9 us

profile of v1, /device:TPU:0, one launch (start us, length us, event | category | flops | bytes accessed | tf_op | source)
XLA Modules:
  0.0 68.9 jit_solution(133518060657192731)
XLA Ops:
  0.6 0.0 copy-start
  0.6 1.2 %copy.19 = bf16[512,2,256]{2,0,1:T(8,128)(2,1)S(1)} copy(bf16[512,2,256]{2,1,0:T(2,128)(2,1)} %param.13) | data formatting | bytes 1048576 | tf_op args[4]
  1.8 0.2 copy-done
  2.0 0.0 copy-start.1
  2.0 1.2 %copy-done.1 = bf16[256,2048]{1,0:T(8,128)(2,1)S(1)} copy-done((bf16[256,2048]{1,0:T(8,128)(2,1)S(1)}, bf16[256,2048]{1,0:T(8,128)(2,1)}, u32[]{:S(2)}) %copy-start.1) | copy-done | bytes 1048600
  3.2 0.0 copy-start.2
  3.2 1.0 %copy-done.2 = bf16[256,1024]{1,0:T(8,128)(2,1)S(1)} copy-done((bf16[256,1024]{1,0:T(8,128)(2,1)S(1)}, bf16[256,1024]{1,0:T(8,128)(2,1)}, u32[]{:S(2)}) %copy-start.2) | copy-done | bytes 524312
  4.3 0.0 copy-start.3
  4.3 1.0 %copy-done.3 = bf16[256,1024]{1,0:T(8,128)(2,1)S(1)} copy-done((bf16[256,1024]{1,0:T(8,128)(2,1)S(1)}, bf16[256,1024]{1,0:T(8,128)(2,1)}, u32[]{:S(2)}) %copy-start.3) | copy-done | bytes 524312
  5.3 0.0 copy-start.4
  5.3 0.9 %copy-done.4 = f32[512,128]{1,0:T(8,128)S(1)} copy-done((f32[512,128]{1,0:T(8,128)S(1)}, f32[512,128]{1,0:T(8,128)}, u32[]{:S(2)}) %copy-start.4) | copy-done | bytes 262168
  6.3 0.0 copy-start.5
  6.3 0.9 %copy-done.5 = f32[128,512]{1,0:T(8,128)S(1)} copy-done((f32[128,512]{1,0:T(8,128)S(1)}, f32[128,512]{1,0:T(8,128)}, u32[]{:S(2)}) %copy-start.5) | copy-done | bytes 262168
  7.2 0.0 copy-start.6
  7.2 0.8 %copy-done.6 = f32[64,2,128]{2,1,0:T(2,128)S(1)} copy-done((f32[64,2,128]{2,1,0:T(2,128)S(1)}, f32[64,2,128]{2,1,0:T(2,128)}, u32[]{:S(2)}) %copy-start.6) | copy-done | bytes 65560
  8.1 0.0 copy-start.7
  8.1 0.8 %copy-done.7 = f32[64,2,128]{2,1,0:T(2,128)S(1)} copy-done((f32[64,2,128]{2,1,0:T(2,128)S(1)}, f32[64,2,128]{2,1,0:T(2,128)}, u32[]{:S(2)}) %copy-start.7) | copy-done | bytes 65560
  8.9 54.3 %shard_map.152 = (f32[128,128]{1,0:T(8,128)S(1)}, f32[128,128]{1,0:T(8,128)S(1)}, f32[512,128]{1,0:T(8,128)S(1)}, f32[128,512]{1,0:T(8,128)S(1)}, f32[512,128]{1...) custom-call(bf16[256,2048]{1,0:T(8,128)(2,1)S(1)} %copy-done, ...), custom_call_target="tpu_custom_call" | custom-call | tf_op jit(solution)/shard_map/pallas_call | solution.py:308
  63.3 0.6 copy.28
  63.9 0.6 copy.29
  64.5 0.7 %copy.30 = f32[512,128]{1,0:T(8,128)} copy(f32[512,128]{1,0:T(8,128)S(1)} %get-tuple-element.34) | data formatting | bytes 524288
  65.2 0.7 %copy.31 = f32[128,512]{1,0:T(8,128)} copy(f32[128,512]{1,0:T(8,128)S(1)} %get-tuple-element.35) | data formatting | bytes 524288
  65.9 0.7 %copy.32 = f32[512,128]{1,0:T(8,128)} copy(f32[512,128]{1,0:T(8,128)S(1)} %get-tuple-element.36) | data formatting | bytes 524288
  66.6 0.7 %copy.33 = f32[128,512]{1,0:T(8,128)} copy(f32[128,512]{1,0:T(8,128)S(1)} %get-tuple-element.37) | data formatting | bytes 524288
  67.3 0.8 %copy.34 = bf16[2048,128]{1,0:T(8,128)(2,1)} copy(bf16[2048,128]{1,0:T(8,128)(2,1)S(1)} %get-tuple-element.38) | data formatting | bytes 1048576
  68.1 0.8 %copy.35 = bf16[128,2048]{1,0:T(8,128)(2,1)} copy(bf16[128,2048]{1,0:T(8,128)(2,1)S(1)} %get-tuple-element.39) | data formatting | bytes 1048576
Async XLA Ops:
  0.6 1.4 %copy-start = (bf16[256,2048]{1,0:T(8,128)(2,1)S(1)}, bf16[256,2048]{1,0:T(8,128)(2,1)}, u32[]{:S(2)}) copy-start(bf16[256,2048]{1,0:T(8,128)(2,1)} %tokens_in.1) | copy-start | bytes 3145732
  2.0 1.2 %copy-start.1 = (bf16[256,2048]{1,0:T(8,128)(2,1)S(1)}, bf16[256,2048]{1,0:T(8,128)(2,1)}, u32[]{:S(2)}) copy-start(bf16[256,2048]{1,0:T(8,128)(2,1)} %block_cot.1) | copy-start | bytes 3145732
  3.2 1.0 %copy-start.2 = (bf16[256,1024]{1,0:T(8,128)(2,1)S(1)}, bf16[256,1024]{1,0:T(8,128)(2,1)}, u32[]{:S(2)}) copy-start(bf16[256,1024]{1,0:T(8,128)(2,1)} %gate_cot.1) | copy-start | bytes 1572868
  4.3 1.0 %copy-start.3 = (bf16[256,1024]{1,0:T(8,128)(2,1)S(1)}, bf16[256,1024]{1,0:T(8,128)(2,1)}, u32[]{:S(2)}) copy-start(bf16[256,1024]{1,0:T(8,128)(2,1)} %conv_out.1) | copy-start | bytes 1572868
  5.3 0.9 %copy-start.4 = (f32[512,128]{1,0:T(8,128)S(1)}, f32[512,128]{1,0:T(8,128)}, u32[]{:S(2)}) copy-start(f32[512,128]{1,0:T(8,128)} %gate_old.1) | copy-start | bytes 786436
  6.3 0.9 %copy-start.5 = (f32[128,512]{1,0:T(8,128)S(1)}, f32[128,512]{1,0:T(8,128)}, u32[]{:S(2)}) copy-start(f32[128,512]{1,0:T(8,128)} %out_old.1) | copy-start | bytes 786436
  7.2 0.8 %copy-start.6 = (f32[64,2,128]{2,1,0:T(2,128)S(1)}, f32[64,2,128]{2,1,0:T(2,128)}, u32[]{:S(2)}) copy-start(f32[64,2,128]{2,1,0:T(2,128)} %param.14) | copy-start | bytes 196612
  8.1 0.8 %copy-start.7 = (f32[64,2,128]{2,1,0:T(2,128)S(1)}, f32[64,2,128]{2,1,0:T(2,128)}, u32[]{:S(2)}) copy-start(f32[64,2,128]{2,1,0:T(2,128)} %param.15) | copy-start | bytes 196612

commit v2 on v1

--- a/solution.py
+++ b/solution.py
@@ -17,30 +17,29 @@
 SLIM = jnp.bfloat16
 
 
-def update_kernel(
+def exchange_kernel(
     fs_total,
     tp_total,
-    clip_level,
     tokens_in,
     gate_cot,
     conv_out,
     block_cot,
     proj,
-    first_old,
-    second_old,
+    first_hbm,
+    second_hbm,
+    gate_hbm,
+    out_hbm,
+    first_new,
+    second_new,
+    dirs,
+    squares,
+    all_proj,
+    gate_slim,
+    out_slim,
     gate_old,
     out_old,
-    first_new,
-    second_new,
-    step_gate,
-    step_out,
-    gate_new,
-    out_new,
-    gate_copy,
-    out_copy,
     left,
     right,
-    peers_proj,
     mix,
     low,
     fs_out,
@@ -48,13 +47,15 @@
     tile_sum,
     tp_out,
     tp_in,
-    dirs,
-    squares,
+    first_old,
+    second_old,
     swap_send,
     swap_recv,
     load_sem,
     proj_send,
     proj_recv,
+    pass_send,
+    pass_recv,
     fs_send,
     fs_recv,
     tp_send,
@@ -109,6 +110,15 @@
     def own_copy(source, target, slot):
         return pltpu.make_async_copy(source, target, load_sem.at[slot])
 
+    loads = (
+        own_copy(gate_hbm, gate_old, 2),
+        own_copy(out_hbm, out_old, 3),
+        own_copy(first_hbm, first_old, 4),
+        own_copy(second_hbm, second_old, 5),
+        own_copy(proj.at[0], all_proj.at[0, me_fs], 6),
+        own_copy(proj.at[1], all_proj.at[1, me_fs], 7),
+    )
+
     @pl.when(core == 0)
     def _():
         own_copy(tokens_in, left.at[0], 0).start()
@@ -118,6 +128,9 @@
     def _():
         own_copy(block_cot, left.at[0], 0).start()
         own_copy(conv_out, right.at[0], 1).start()
+
+    for load in loads:
+        load.start()
 
     barrier = pltpu.get_barrier_semaphore()
     for step in range(1, fs_total):
@@ -132,7 +145,7 @@
 
     proj_copies = [None]
     for step in range(1, fs_total):
-        copy = send_fs(proj.at[core], peers_proj.at[step], proj_send, proj_recv, step)
+        copy = send_fs(proj.at[core], all_proj.at[core, me_fs], proj_send, proj_recv, step)
         copy.start()
         proj_copies.append(copy)
 
@@ -157,10 +170,16 @@
         part = left[:, :, columns].reshape(2 * local, rows_d)
         return jnp.dot(part, factor_rows, preferred_element_type=WIDE)
 
+    pass_copies = [None]
     mix[...] = mixed(me_fs, proj[core])
     for step in range(1, fs_total):
         proj_copies[step].wait_recv()
-        mix[...] += mixed(fs_source(step), peers_proj[step])
+        source = fs_source(step)
+        block = all_proj.at[core, source]
+        copy = send_tp(block, block, pass_send, pass_recv, step, partner)
+        copy.start()
+        pass_copies.append(copy)
+        mix[...] += mixed(source, all_proj[core, source])
 
     own_copy(gate_cot, right.at[0], 1).wait()
     swap_right.wait_recv()
@@ -183,6 +202,16 @@
         copy = send_fs(fs_out.at[step], fs_in.at[step], fs_send, fs_recv, step)
         copy.start()
         fs_copies.append(copy)
+    loads[0].wait()
+    loads[1].wait()
+    gate_slim[me_fs] = gate_old[...].astype(SLIM)
+    out_slim[me_fs] = out_old[...].astype(SLIM)
+    last_copies = []
+    for step in range(1, fs_total):
+        block = gate_slim.at[me_fs]
+        copy = send_fs(block, block, gate_send, gate_recv, step)
+        copy.start()
+        last_copies.append(copy)
     rows = low_rows(me_fs)
     for tile in range(tp_total):
         tile_sum[tile] = rows[:, tile * width : (tile + 1) * width]
@@ -206,6 +235,8 @@
         else:
             other = piece if other is None else other + piece
 
+    loads[2].wait()
+    loads[3].wait()
     lows = (jnp.where(core == 0, same, other), jnp.where(core == 0, other, same))
     for index in range(2):
         picked = pl.ds(index, rank_rows, stride=2)
@@ -220,6 +251,11 @@
         copy = send_fs(dirs.at[me_fs], dirs.at[me_fs], dir_send, dir_recv, step)
         copy.start()
         dir_copies.append(copy)
+    for step in range(1, fs_total):
+        block = out_slim.at[me_fs]
+        copy = send_fs(block, block, out_send, out_recv, step)
+        copy.start()
+        last_copies.append(copy)
     for step in range(1, fs_total):
         dir_copies[step].wait_recv()
 
@@ -236,47 +272,104 @@
         )
         copy.start()
         square_copies.append(copy)
-    raw_gate = jnp.dot(proj[0], gate_dir, preferred_element_type=WIDE)
-    raw_out = lax.dot_general(
-        flip_dir, proj[1], (((0,), (1,)), ((), ())), preferred_element_type=WIDE
-    )
     for step in range(1, tp_total):
-        square_copies[step].wait_recv()
-    totals = jnp.sum(squares[...], axis=0)
-    gate_norm = jnp.sqrt(jnp.sum(totals[0], keepdims=True))
-    flip_norm = jnp.sqrt(jnp.sum(totals[1], keepdims=True))
-    scaled_gate = raw_gate * (clip_level / jnp.maximum(gate_norm, clip_level))
-    scaled_out = raw_out * (clip_level / jnp.maximum(flip_norm, clip_level))
-    step_gate[...] = scaled_gate
-    step_out[...] = scaled_out
-    fresh_gate = gate_old[...] - LEARN_RATE * scaled_gate
-    fresh_out = out_old[...] - LEARN_RATE * scaled_out
-    own_rows = pl.ds(pl.multiple_of(me_fs * rows_d, 128), rows_d)
-    gate_copy[own_rows, :] = fresh_gate.astype(SLIM)
-    out_copy[:, own_rows] = fresh_out.astype(SLIM)
-    gate_block = gate_copy.at[own_rows, :]
-    out_block = out_copy.at[:, own_rows]
-    last_copies = []
-    for step in range(1, fs_total):
-        copy = send_fs(gate_block, gate_block, gate_send, gate_recv, step)
-        copy.start()
-        last_copies.append(copy)
-        copy = send_fs(out_block, out_block, out_send, out_recv, step)
-        copy.start()
-        last_copies.append(copy)
-    gate_new[...] = fresh_gate
-    out_new[...] = fresh_out
+        square_copies[step].wait()
+        tp_copies[step].wait_send()
     for step in range(1, fs_total):
         proj_copies[step].wait_send()
+        pass_copies[step].wait()
         fs_copies[step].wait_send()
         dir_copies[step].wait_send()
-    for step in range(1, tp_total):
-        tp_copies[step].wait_send()
-        square_copies[step].wait_send()
+    loads[4].wait()
+    loads[5].wait()
     swap_left.wait_send()
     swap_right.wait_send()
     for copy in last_copies:
         copy.wait()
+
+
+def finish_kernel(
+    clip_level,
+    first_in,
+    second_in,
+    dirs,
+    squares,
+    all_proj,
+    gate_slim,
+    out_slim,
+    gate_old,
+    out_old,
+    first_new,
+    second_new,
+    step_gate,
+    step_out,
+    gate_new,
+    out_new,
+    gate_copy,
+    out_copy,
+    gate_step,
+    out_step,
+    gate_fresh,
+    out_fresh,
+    gate_round,
+    out_round,
+    sems,
+):
+    me_fs = lax.axis_index("fs")
+    fs_total, _, rank_rows, width = dirs.shape
+    rank = fs_total * rank_rows
+    rows_d = all_proj.shape[2]
+    stores = []
+
+    def store(source, target):
+        copy = pltpu.make_async_copy(source, target, sems.at[len(stores)])
+        copy.start()
+        stores.append(copy)
+
+    store(first_in, first_new)
+    store(second_in, second_new)
+    totals = jnp.sum(squares[...], axis=0)
+    gate_norm = jnp.sqrt(jnp.sum(totals[0], keepdims=True))
+    flip_norm = jnp.sqrt(jnp.sum(totals[1], keepdims=True))
+    gate_factor = clip_level / jnp.maximum(gate_norm, clip_level)
+    out_factor = clip_level / jnp.maximum(flip_norm, clip_level)
+    gate_dir = dirs[:, 0].reshape(rank, width)
+    flip_dir = dirs[:, 1].reshape(rank, width)
+
+    def gate_rows(block):
+        return gate_factor * jnp.dot(all_proj[0, block], gate_dir, preferred_element_type=WIDE)
+
+    def out_columns(block):
+        return out_factor * lax.dot_general(
+            flip_dir, all_proj[1, block], (((0,), (1,)), ((), ())), preferred_element_type=WIDE
+        )
+
+    for block in range(fs_total):
+        part = pl.ds(block * rows_d, rows_d)
+        fresh = gate_slim[block].astype(WIDE) - LEARN_RATE * gate_rows(block)
+        gate_round[part, :] = fresh.astype(SLIM)
+    store(gate_round, gate_copy)
+    for block in range(fs_total):
+        part = pl.ds(block * rows_d, rows_d)
+        fresh = out_slim[block].astype(WIDE) - LEARN_RATE * out_columns(block)
+        out_round[:, part] = fresh.astype(SLIM)
+    store(out_round, out_copy)
+    scaled = gate_rows(me_fs)
+    gate_step[...] = scaled
+    store(gate_step, step_gate)
+    gate_fresh[...] = gate_old[...] - LEARN_RATE * scaled
+    store(gate_fresh, gate_new)
+    scaled = out_columns(me_fs)
+    out_step[...] = scaled
+    store(out_step, step_out)
+    out_fresh[...] = out_old[...] - LEARN_RATE * scaled
+    store(out_fresh, out_new)
+    for copy in stores:
+        copy.wait()
+
+
+def held(array):
+    return pltpu.with_memory_space_constraint(array, pltpu.HBM)
 
 
 def shards(
@@ -301,12 +394,62 @@
     flat = (2 * rank_rows, width)
     shape = jax.ShapeDtypeStruct
     whole = pl.BlockSpec(memory_space=pltpu.VMEM)
-    away = pl.BlockSpec(memory_space=pl.ANY)
+    away = pl.BlockSpec(memory_space=pltpu.HBM)
     fs_sems = pltpu.SemaphoreType.DMA((fs_total,))
     tp_sems = pltpu.SemaphoreType.DMA((tp_total,))
     two_sems = pltpu.SemaphoreType.DMA((2,))
+    middle = pl.pallas_call(
+        functools.partial(exchange_kernel, fs_total, tp_total),
+        out_shape=(
+            shape(flat, WIDE),
+            shape(flat, WIDE),
+            shape((fs_total, 2, rank_rows, width), SLIM),
+            shape((tp_total, 2, 8, width), WIDE),
+            shape((2, fs_total, rows_d, rank), SLIM),
+            shape((fs_total, rows_d, width), SLIM),
+            shape((fs_total, width, rows_d), SLIM),
+            shape((rows_d, width), WIDE),
+            shape((width, rows_d), WIDE),
+        ),
+        in_specs=[away] * 4 + [whole] + [away] * 4,
+        out_specs=(whole,) * 9,
+        scratch_shapes=[
+            pltpu.VMEM((2, local, model), SLIM),
+            pltpu.VMEM((2, local, channels), SLIM),
+            pltpu.VMEM((2 * local, rank), WIDE),
+            pltpu.VMEM((rank, channels), WIDE),
+            pltpu.VMEM((fs_total, tp_total, rank_rows, width), SLIM),
+            pltpu.VMEM((fs_total, tp_total, rank_rows, width), SLIM),
+            pltpu.VMEM((tp_total, rank_rows, width), WIDE),
+            pltpu.VMEM((tp_total, rank_rows, width), SLIM),
+            pltpu.VMEM((tp_total, rank_rows, width), SLIM),
+            pltpu.VMEM(flat, WIDE),
+            pltpu.VMEM(flat, WIDE),
+            two_sems,
+            two_sems,
+            pltpu.SemaphoreType.DMA((8,)),
+        ]
+        + [fs_sems] * 6
+        + [tp_sems] * 2
+        + [fs_sems] * 2
+        + [tp_sems] * 2
+        + [fs_sems] * 4,
+        compiler_params=pltpu.CompilerParams(
+            collective_id=0, has_side_effects=True, vmem_limit_bytes=30 * 1024 * 1024
+        ),
+    )(
+        held(tokens_in),
+        held(gate_cotangent),
+        held(conv_output),
+        held(block_cotangent),
+        proj,
+        held(first_moment.reshape(flat)),
+        held(second_moment.reshape(flat)),
+        held(gate_master),
+        held(out_master),
+    )
     results = pl.pallas_call(
-        functools.partial(update_kernel, fs_total, tp_total, clip_level),
+        functools.partial(finish_kernel, clip_level),
         out_shape=(
             shape(flat, WIDE),
             shape(flat, WIDE),
@@ -317,53 +460,19 @@
             shape((model, width), SLIM),
             shape((width, model), SLIM),
         ),
-        in_specs=[away] * 4 + [whole] * 5,
-        out_specs=(whole,) * 8,
+        in_specs=[whole] * 9,
+        out_specs=(away,) * 8,
         scratch_shapes=[
-            pltpu.VMEM((2, local, model), SLIM),
-            pltpu.VMEM((2, local, channels), SLIM),
-            pltpu.VMEM((fs_total, rows_d, rank), SLIM),
-            pltpu.VMEM((2 * local, rank), WIDE),
-            pltpu.VMEM((rank, channels), WIDE),
-            pltpu.VMEM((fs_total, tp_total, rank_rows, width), SLIM),
-            pltpu.VMEM((fs_total, tp_total, rank_rows, width), SLIM),
-            pltpu.VMEM((tp_total, rank_rows, width), WIDE),
-            pltpu.VMEM((tp_total, rank_rows, width), SLIM),
-            pltpu.VMEM((tp_total, rank_rows, width), SLIM),
-            pltpu.VMEM((fs_total, 2, rank_rows, width), SLIM),
-            pltpu.VMEM((tp_total, 2, 8, width), WIDE),
-            two_sems,
-            two_sems,
-            two_sems,
-            fs_sems,
-            fs_sems,
-            fs_sems,
-            fs_sems,
-            tp_sems,
-            tp_sems,
-            fs_sems,
-            fs_sems,
-            tp_sems,
-            tp_sems,
-            fs_sems,
-            fs_sems,
-            fs_sems,
-            fs_sems,
+            pltpu.VMEM((rows_d, width), WIDE),
+            pltpu.VMEM((width, rows_d), WIDE),
+            pltpu.VMEM((rows_d, width), WIDE),
+            pltpu.VMEM((width, rows_d), WIDE),
+            pltpu.VMEM((model, width), SLIM),
+            pltpu.VMEM((width, model), SLIM),
+            pltpu.SemaphoreType.DMA((8,)),
         ],
-        compiler_params=pltpu.CompilerParams(
-            collective_id=0, has_side_effects=True, vmem_limit_bytes=40 * 1024 * 1024
-        ),
-    )(
-        tokens_in,
-        gate_cotangent,
-        conv_output,
-        block_cotangent,
-        proj,
-        first_moment.reshape(flat),
-        second_moment.reshape(flat),
-        gate_master,
-        out_master,
-    )
+        compiler_params=pltpu.CompilerParams(vmem_limit_bytes=30 * 1024 * 1024),
+    )(*middle)
     first_new, second_new = (part.reshape(rank_rows, 2, width) for part in results[:2])
     return (first_new, second_new) + tuple(results[2:])
 

time: 69.4 us -> 48.6 us (0.70)
  local copies, waits for them, and re-layouts: 13.9 us -> 1.11 us
  Pallas kernels: 54.3 us -> 46.7 us
    unnamed x25 -> x1, local copies, waits for them, and re-layouts: 13.9 us -> 1.11 us
    pallas_call x1 -> x2, Pallas kernels: 54.3 us -> 46.7 us  [the longest x1 44.7 us: shards(): pl.pallas_call(functools.partial(exchange_kernel, fs_total, tp_total), ou...]
where the time goes in v2:
time: 48.6 us; the launch traced here: 48.5 us
  Pallas kernels  46.7 us (96%)
  local copies, waits for them, and re-layouts  1.11 us (2%)
  between operations  0.64 us (1%)
    pallas_call x1, Pallas kernels, shards(): pl.pallas_call(functools.partial(exchange_kernel, fs_total, tp_total), ou...  44.7 us
    pallas_call x1, Pallas kernels, shards(): pl.pallas_call(functools.partial(finish_kernel, clip_level), out_shape=(s...  2.02 us
    unnamed x1, local copies, waits for them, and re-layouts  1.11 us

profile of v2, /device:TPU:0, one launch (start us, length us, event | category | flops | bytes accessed | tf_op | source)
XLA Modules:
  0.0 48.5 jit_solution(7707748762828951854)
XLA Ops:
  0.6 1.1 %copy.19 = bf16[512,2,256]{2,0,1:T(8,128)(2,1)S(1)} copy(bf16[512,2,256]{2,1,0:T(2,128)(2,1)} %param.13) | data formatting | bytes 1048576 | tf_op args[4]
  1.7 44.7 %shard_map.152 = (f32[128,128]{1,0:T(8,128)S(1)}, f32[128,128]{1,0:T(8,128)S(1)}, bf16[4,2,64,128]{3,2,1,0:T(8,128)(2,1)S(1)}, f32[8,2,8,128]{3,2,1,0:T(8,128)S(...) custom-call(bf16[256,2048]{1,0:T(8,128)(2,1)} %tokens_in.1, ...), custom_call_target="tpu_custom_call" | custom-call | tf_op jit(solution)/shard_map/pallas_call | solution.py:401
  46.5 2.0 %shard_map.153 = (f32[128,128]{1,0:T(8,128)}, f32[128,128]{1,0:T(8,128)}, f32[512,128]{1,0:T(8,128)}, f32[128,512]{1,0:T(8,128)}, f32[512,128]{1,0:T(8,128)}, /*...) custom-call(f32[128,128]{1,0:T(8,128)S(1)} %get-tuple-element.25.first_in, ...), custom_call_target="tpu_custom_call" | custom-call | tf_op jit(solution)/shard_map/pallas_call | solution.py:451

commit v3 on v2

--- a/solution.py
+++ b/solution.py
@@ -49,6 +49,7 @@
     tp_in,
     first_old,
     second_old,
+    tp_squares,
     swap_send,
     swap_recv,
     load_sem,
@@ -68,6 +69,8 @@
     gate_recv,
     out_send,
     out_recv,
+    sum_send,
+    sum_recv,
 ):
     me_fs = lax.axis_index("fs")
     me_tp = lax.axis_index("tp")
@@ -143,11 +146,38 @@
         )
     pl.semaphore_wait(barrier, fs_total + tp_total - 2)
 
-    proj_copies = [None]
-    for step in range(1, fs_total):
-        copy = send_fs(proj.at[core], all_proj.at[core, me_fs], proj_send, proj_recv, step)
-        copy.start()
-        proj_copies.append(copy)
+    quad = fs_total == 4
+    beside = me_fs + 1 - 2 * lax.rem(me_fs, 2)
+    above = lax.rem(me_fs + 2, fs_total)
+    half = rows_d // 2
+
+    def send_half(target, owner, part, index):
+        rows = pl.ds(part * half, half)
+        block = all_proj.at[core, owner, rows]
+        mine = owner is me_fs
+        return pltpu.make_async_remote_copy(
+            src_ref=proj.at[core, rows] if mine else block,
+            dst_ref=block,
+            send_sem=proj_send.at[index],
+            recv_sem=proj_recv.at[index],
+            device_id={"fs": target, "tp": me_tp},
+            device_id_type=MESH_ID,
+        )
+
+    proj_copies = []
+    if quad:
+        plan = ((beside, 0), (above, 1), (beside, 1), (above, 0))
+        for index, (target, part) in enumerate(plan):
+            copy = send_half(target, me_fs, part, index)
+            copy.start()
+            proj_copies.append(copy)
+    else:
+        for step in range(1, fs_total):
+            copy = send_fs(
+                proj.at[core], all_proj.at[core, me_fs], proj_send, proj_recv, step
+            )
+            copy.start()
+            proj_copies.append(copy)
 
     swap_left = send_tp(block_cot, left.at[1], swap_send, swap_recv, 0, partner)
     swap_right = send_tp(conv_out, right.at[1], swap_send, swap_recv, 1, partner)
@@ -170,16 +200,47 @@
         part = left[:, :, columns].reshape(2 * local, rows_d)
         return jnp.dot(part, factor_rows, preferred_element_type=WIDE)
 
-    pass_copies = [None]
     mix[...] = mixed(me_fs, proj[core])
-    for step in range(1, fs_total):
-        proj_copies[step].wait_recv()
-        source = fs_source(step)
+    loads[0].wait()
+    gate_slim[me_fs] = gate_old[...].astype(SLIM)
+    last_copies = []
+    pass_copies = []
+
+    def send_gate():
+        for step in range(1, fs_total):
+            block = gate_slim.at[me_fs]
+            copy = send_fs(block, block, gate_send, gate_recv, step)
+            copy.start()
+            last_copies.append(copy)
+
+    def absorb(source):
         block = all_proj.at[core, source]
+        step = len(pass_copies) + 1
         copy = send_tp(block, block, pass_send, pass_recv, step, partner)
         copy.start()
         pass_copies.append(copy)
         mix[...] += mixed(source, all_proj[core, source])
+
+    if quad:
+        for index, (target, owner, part) in enumerate(((above, beside, 0), (beside, above, 1))):
+            proj_copies[index].wait_recv()
+            copy = send_half(target, owner, part, index + 4)
+            copy.start()
+            proj_copies.append(copy)
+        send_gate()
+        proj_copies[2].wait_recv()
+        absorb(beside)
+        proj_copies[3].wait_recv()
+        absorb(above)
+        proj_copies[4].wait_recv()
+        proj_copies[5].wait_recv()
+        absorb(fs_total - 1 - me_fs)
+    else:
+        for step in range(1, fs_total):
+            proj_copies[step - 1].wait_recv()
+            if step == fs_total - 1:
+                send_gate()
+            absorb(fs_source(step))
 
     own_copy(gate_cot, right.at[0], 1).wait()
     swap_right.wait_recv()
@@ -202,14 +263,11 @@
         copy = send_fs(fs_out.at[step], fs_in.at[step], fs_send, fs_recv, step)
         copy.start()
         fs_copies.append(copy)
-    loads[0].wait()
     loads[1].wait()
-    gate_slim[me_fs] = gate_old[...].astype(SLIM)
     out_slim[me_fs] = out_old[...].astype(SLIM)
-    last_copies = []
-    for step in range(1, fs_total):
-        block = gate_slim.at[me_fs]
-        copy = send_fs(block, block, gate_send, gate_recv, step)
+    for step in range(1, fs_total):
+        block = out_slim.at[me_fs]
+        copy = send_fs(block, block, out_send, out_recv, step)
         copy.start()
         last_copies.append(copy)
     rows = low_rows(me_fs)
@@ -244,42 +302,42 @@
         second = BETA_SECOND * second_old[picked, :] + (1.0 - BETA_SECOND) * lows[index] * lows[index]
         first_new[picked, :] = first
         second_new[picked, :] = second
-        dirs[me_fs, index] = (first / jnp.sqrt(second)).astype(SLIM)
+        direction = first / jnp.sqrt(second)
+        dirs[me_fs, index] = direction.astype(SLIM)
+        tp_squares[0, index] = jnp.sum(
+            (direction * direction).reshape(rank_rows // 8, 8, width), axis=0
+        )
 
     dir_copies = [None]
     for step in range(1, fs_total):
         copy = send_fs(dirs.at[me_fs], dirs.at[me_fs], dir_send, dir_recv, step)
         copy.start()
         dir_copies.append(copy)
-    for step in range(1, fs_total):
-        block = out_slim.at[me_fs]
-        copy = send_fs(block, block, out_send, out_recv, step)
-        copy.start()
-        last_copies.append(copy)
-    for step in range(1, fs_total):
-        dir_copies[step].wait_recv()
-
-    gate_dir = dirs[:, 0].reshape(rank, width)
-    flip_dir = dirs[:, 1].reshape(rank, width)
-    gate_wide = gate_dir.astype(WIDE)
-    flip_wide = flip_dir.astype(WIDE)
-    squares[0, 0] = jnp.sum((gate_wide * gate_wide).reshape(rank // 8, 8, width), axis=0)
-    squares[0, 1] = jnp.sum((flip_wide * flip_wide).reshape(rank // 8, 8, width), axis=0)
-    square_copies = [None]
+    square_copies = []
     for step in range(1, tp_total):
         copy = send_tp(
-            squares.at[0], squares.at[step], square_send, square_recv, step, tp_peer(step)
+            tp_squares.at[0], tp_squares.at[step], square_send, square_recv, step, tp_peer(step)
         )
         copy.start()
         square_copies.append(copy)
+    for copy in square_copies:
+        copy.wait_recv()
+    squares[me_fs] = jnp.sum(tp_squares[...], axis=0)
+    sum_copies = []
+    for step in range(1, fs_total):
+        block = squares.at[me_fs]
+        copy = send_fs(block, block, sum_send, sum_recv, step)
+        copy.start()
+        sum_copies.append(copy)
+    for copy in square_copies + proj_copies:
+        copy.wait_send()
+    for copy in pass_copies + sum_copies:
+        copy.wait()
     for step in range(1, tp_total):
-        square_copies[step].wait()
         tp_copies[step].wait_send()
     for step in range(1, fs_total):
-        proj_copies[step].wait_send()
-        pass_copies[step].wait()
         fs_copies[step].wait_send()
-        dir_copies[step].wait_send()
+        dir_copies[step].wait()
     loads[4].wait()
     loads[5].wait()
     swap_left.wait_send()
@@ -404,7 +462,7 @@
             shape(flat, WIDE),
             shape(flat, WIDE),
             shape((fs_total, 2, rank_rows, width), SLIM),
-            shape((tp_total, 2, 8, width), WIDE),
+            shape((fs_total, 2, 8, width), WIDE),
             shape((2, fs_total, rows_d, rank), SLIM),
             shape((fs_total, rows_d, width), SLIM),
             shape((fs_total, width, rows_d), SLIM),
@@ -425,15 +483,17 @@
             pltpu.VMEM((tp_total, rank_rows, width), SLIM),
             pltpu.VMEM(flat, WIDE),
             pltpu.VMEM(flat, WIDE),
+            pltpu.VMEM((tp_total, 2, 8, width), WIDE),
             two_sems,
             two_sems,
             pltpu.SemaphoreType.DMA((8,)),
         ]
-        + [fs_sems] * 6
+        + [pltpu.SemaphoreType.DMA((fs_total + 2,))] * 2
+        + [fs_sems] * 4
         + [tp_sems] * 2
         + [fs_sems] * 2
         + [tp_sems] * 2
-        + [fs_sems] * 4,
+        + [fs_sems] * 6,
         compiler_params=pltpu.CompilerParams(
             collective_id=0, has_side_effects=True, vmem_limit_bytes=30 * 1024 * 1024
         ),

time: 48.6 us -> 44.8 us (0.922)
  Pallas kernels: 46.7 us -> 42.9 us
    pallas_call x1, Pallas kernels: 44.7 us -> 40.8 us  [shards(): pl.pallas_call(functools.partial(exchange_kernel, fs_total, tp_total), ou...]
where the time goes in v3:
time: 44.8 us; the launch traced here: 44.6 us
  Pallas kernels  42.9 us (96%)
  local copies, waits for them, and re-layouts  1.11 us (2%)
  between operations  0.64 us (1%)
    pallas_call x1, Pallas kernels, shards(): pl.pallas_call(functools.partial(exchange_kernel, fs_total, tp_total), ou...  40.8 us
    pallas_call x1, Pallas kernels, shards(): pl.pallas_call(functools.partial(finish_kernel, clip_level), out_shape=(s...  2.02 us
    unnamed x1, local copies, waits for them, and re-layouts  1.11 us

profile of v3, /device:TPU:0, one launch (start us, length us, event | category | flops | bytes accessed | tf_op | source)
XLA Modules:
  0.0 44.6 jit_solution(2209734536874744604)
XLA Ops:
  0.6 1.1 %copy.19 = bf16[512,2,256]{2,0,1:T(8,128)(2,1)S(1)} copy(bf16[512,2,256]{2,1,0:T(2,128)(2,1)} %param.13) | data formatting | bytes 1048576 | tf_op args[4]
  1.7 40.8 %shard_map.152 = (f32[128,128]{1,0:T(8,128)S(1)}, f32[128,128]{1,0:T(8,128)S(1)}, bf16[4,2,64,128]{3,2,1,0:T(8,128)(2,1)S(1)}, f32[4,2,8,128]{3,2,1,0:T(8,128)S(...) custom-call(bf16[256,2048]{1,0:T(8,128)(2,1)} %tokens_in.1, ...), custom_call_target="tpu_custom_call" | custom-call | tf_op jit(solution)/shard_map/pallas_call | solution.py:459
  42.6 2.0 %shard_map.153 = (f32[128,128]{1,0:T(8,128)}, f32[128,128]{1,0:T(8,128)}, f32[512,128]{1,0:T(8,128)}, f32[128,512]{1,0:T(8,128)}, f32[512,128]{1,0:T(8,128)}, /*...) custom-call(f32[128,128]{1,0:T(8,128)S(1)} %get-tuple-element.25.first_in, ...), custom_call_target="tpu_custom_call" | custom-call | tf_op jit(solution)/shard_map/pallas_call | solution.py:511
